TPU v7x, 512 devices: a whole 4x4x16 slice. The times are simulated.
512 devices in a mesh: sp: 32 (over z, core), tp: 16 (over y, x).
Axes of the slice: x: 4, y: 4, z: 16, core: 2. Of those that a mesh axis runs over, the one named last changes fastest.
Arguments:
- query_a: bfloat16 [6144, 2048], P('sp', 'tp'), may hold values from -6 to 6
- key_a: bfloat16 [6144, 2048], P('sp', 'tp'), may hold values from -6 to 6
- value_a: bfloat16 [6144, 2048], P('sp', 'tp'), may hold values from -6 to 6
- query_b: bfloat16 [6144, 2048], P('sp', 'tp'), may hold values from -6 to 6
- key_b: bfloat16 [6144, 2048], P('sp', 'tp'), may hold values from -6 to 6
- value_b: bfloat16 [6144, 2048], P('sp', 'tp'), may hold values from -6 to 6
- stop_a: float32 [6144, 32], P('sp', 'tp'), may hold values from -14 to -1
- stop_b: float32 [6144, 16], P('sp', 'tp'), may hold values from -14 to -1
- out_a: bfloat16 [2048, 2048], P('tp'), may hold values from -4 to 4
- out_b: bfloat16 [2048, 2048], P('tp'), may hold values from -4 to 4
- resid: bfloat16 [6144, 2048], P('sp', 'tp'), may hold values from -20 to 20
- mix_gain: float32 [2048], P('tp'), may hold values from 0.1 to 1.9
- ffn_gain: float32 [2048], P('tp'), may hold values from 0.1 to 1.9
- routes: int32 [6144, 2], P('sp'), may hold values from 0 to 127, all different within a row; in each aligned block of 192 rows (0 to 191, 192 to 383, ...) at most 5 rows name the same one
- gates: float32 [6144, 2], P('sp'), may hold values from 0.25 to 1.5
- exp_gate: bfloat16 [128, 2048, 512], P('sp', 'tp'), may hold values from -0.125 to 0.125
- exp_up: bfloat16 [128, 2048, 512], P('sp', 'tp'), may hold values from -0.125 to 0.125
- exp_down: bfloat16 [128, 512, 2048], P('sp', None, 'tp'), may hold values from -0.25 to 0.25
- sh_gate: bfloat16 [2048, 512], P('tp'), may hold values from -0.125 to 0.125
- sh_up: bfloat16 [2048, 512], P('tp'), may hold values from -0.125 to 0.125
- sh_down: bfloat16 [512, 2048], P(None, 'tp'), may hold values from -4 to 4
Outputs:
- result: bfloat16 [6144, 2048], P('sp', 'tp')
Inputs may be any that keep to these rules, and one draw needn't show every extreme that they name: `routes`: each row names 2 different experts. Within the rows of one index of sp (aligned blocks of 192 rows) no expert is named by more than 5 rows, a bound that some block reaches.
All inputs are finite; a program needn't handle non-finite values.
Results may differ from a plain program's by a relative error of at most 0.02.
Values may be sent and summed in bfloat16 or wider, within the bound.
A program may use at most 64 MiB of HBM per device.

v0:
```python
import jax
import jax.numpy as jnp
from jax import lax
from jax.sharding import Mesh
from jax.sharding import PartitionSpec as P

D = 2048
TP = ("tp_0", "tp_1")
epsilon = 1e-06


def cut_along(x, dim, size):
    before, after = (x.shape[:dim], x.shape[dim + 1 :])
    return jnp.moveaxis(x.reshape(*before, size, -1, *after), dim, 0)


def sum_at_owner(x, axis, dim):
    tiles = cut_along(x, dim, lax.axis_size(axis))
    arrived = lax.all_to_all(tiles, axis, split_axis=0, concat_axis=0, tiled=True)
    return arrived.astype(jnp.float32).sum(axis=0)


def by_axis(x, axes):
    for axis in axes:
        x = lax.psum(x, axis)
    return x


def suffix_sums(failing):
    width = failing.shape[-1]
    pieces = width // width
    shaped = failing.reshape(failing.shape[:-1] + (pieces, width))
    places = jnp.arange(width)
    upper = (places[:, None] > places[None, :]).astype(jnp.float32)
    inner = jnp.matmul(shaped, upper)
    return inner.reshape(failing.shape)


def stick_block(state, queries, keyset, causal):
    outputs, carried = state
    new_out = []
    new_carry = []
    for group in range(2):
        query, stop, scale = queries[group]
        keys = keyset[2 * group]
        values = keyset[2 * group + 1]
        scores = jnp.einsum("qhd,khd->hqk", query, keys, preferred_element_type=jnp.float32)
        scores = scores * scale + jnp.transpose(stop)[:, :, None]
        failing = jax.nn.log_sigmoid(-scores)
        if causal is not None:
            failing = jnp.where(causal, failing, 0.0)
        after = suffix_sums(failing) + carried[group][:, :, None]
        weight = jnp.exp(jax.nn.log_sigmoid(scores) + after)
        if causal is not None:
            weight = jnp.where(causal, weight, 0.0)
        added = jnp.einsum(
            "hqk,khe->qhe", weight.astype(jnp.bfloat16), values, preferred_element_type=jnp.float32
        )
        new_out.append(outputs[group] + added)
        new_carry.append(carried[group] + jnp.sum(failing, axis=-1))
    return (tuple(new_out), tuple(new_carry))


def empty_state(count, heads_a, size_a, heads_b, size_b):
    return (
        (
            jnp.zeros((count, heads_a, size_a), jnp.float32),
            jnp.zeros((count, heads_b, size_b), jnp.float32),
        ),
        (jnp.zeros((heads_a, count), jnp.float32), jnp.zeros((heads_b, count), jnp.float32)),
    )


def joined_rows(state, width_a, width_b):
    count = state[0][0].shape[0]
    return jnp.concatenate(
        [
            state[0][0].astype(jnp.bfloat16).reshape(count, width_a),
            state[0][1].astype(jnp.bfloat16).reshape(count, width_b),
        ],
        axis=1,
    )


def shards(
    query_a,
    key_a,
    value_a,
    query_b,
    key_b,
    value_b,
    stop_a,
    stop_b,
    out_a,
    out_b,
    resid,
    mix_gain,
    ffn_gain,
    routes,
    gates,
    exp_gate,
    exp_up,
    exp_down,
    sh_gate,
    sh_up,
    sh_down,
):
    rows = query_a.shape[0]
    heads_a = stop_a.shape[1]
    heads_b = stop_b.shape[1]
    width_a = query_a.shape[1]
    width_b = query_b.shape[1]
    size_a = width_a // heads_a
    size_b = width_b // heads_b

    def unpack(joined):
        count = joined.shape[0]
        return (
            joined[:, :width_a].reshape(count, heads_a, size_a),
            joined[:, width_a : 2 * width_a].reshape(count, heads_a, size_a),
            joined[:, 2 * width_a : 2 * width_a + width_b].reshape(count, heads_b, size_b),
            joined[:, 2 * width_a + width_b :].reshape(count, heads_b, size_b),
        )

    joined_local = jnp.concatenate([key_a, value_a, key_b, value_b], axis=1)
    places = jnp.arange(rows)
    position = lax.axis_index("sp")
    n_sp = lax.axis_size("sp")
    count = query_a.shape[0]
    queries = (
        (query_a.reshape(count, heads_a, size_a), stop_a, size_a ** (-0.5)),
        (query_b.reshape(count, heads_b, size_b), stop_b, size_b ** (-0.5)),
    )
    causal = (places[None, :] < places[:, None])[None]
    state = stick_block(
        empty_state(rows, heads_a, size_a, heads_b, size_b), queries, unpack(joined_local), causal
    )
    gathered = lax.all_gather(joined_local, "sp", axis=0, tiled=True)

    def turn(step, inner_state):
        start = jnp.maximum(position - step, 0) * rows
        piece = lax.dynamic_slice_in_dim(gathered, start, rows, 0)
        return lax.cond(
            position >= step,
            lambda inputs: stick_block(inputs, queries, unpack(piece), None),
            lambda inputs: inputs,
            inner_state,
        )

    state = lax.fori_loop(1, n_sp, turn, state)
    attended = joined_rows(state, width_a, width_b)
    attended_a = attended[:, :width_a]
    attended_b = attended[:, width_a:]
    partial_value = jnp.dot(attended_a, out_a, preferred_element_type=jnp.float32)
    partial_value = partial_value + jnp.dot(attended_b, out_b, preferred_element_type=jnp.float32)
    mixed = sum_at_owner(partial_value.astype(jnp.bfloat16), TP, 1)
    mix_total = by_axis(jnp.sum(mixed * mixed, axis=1), TP)
    branch = mixed * lax.rsqrt(mix_total / D + epsilon)[:, None] * mix_gain[None, :]
    stream = lax.optimization_barrier((resid.astype(jnp.float32) + branch).astype(jnp.bfloat16))
    stream_f = stream.astype(jnp.float32)
    ffn_total = by_axis(jnp.sum(stream_f * stream_f, axis=1), TP)
    normed = (stream_f * lax.rsqrt(ffn_total / D + epsilon)[:, None] * ffn_gain[None, :]).astype(
        jnp.bfloat16
    )
    shared_gate, shared_up = (
        lax.psum(
            jnp.dot(normed, sh_gate, preferred_element_type=jnp.float32).astype(jnp.bfloat16), TP
        ).astype(jnp.float32),
        lax.psum(
            jnp.dot(normed, sh_up, preferred_element_type=jnp.float32).astype(jnp.bfloat16), TP
        ).astype(jnp.float32),
    )
    shared_hidden = (jax.nn.silu(shared_gate) * shared_up).astype(jnp.bfloat16)
    shared_out = jnp.dot(shared_hidden, sh_down, preferred_element_type=jnp.float32)
    local_experts = exp_gate.shape[0]
    experts = local_experts * n_sp
    top_count = routes.shape[1]
    capacity = max(1, (3 * rows * top_count + 2 * experts - 1) // (2 * experts))
    flat_routes = routes.reshape(-1)
    onehot = (flat_routes[:, None] == jnp.arange(experts, dtype=jnp.int32)[None, :]).astype(
        jnp.int32
    )
    earlier = jnp.cumsum(onehot, axis=0) - onehot
    slot = flat_routes * capacity + jnp.sum(earlier * onehot, axis=1)
    chooser = (slot[:, None] == jnp.arange(experts * capacity, dtype=jnp.int32)[None, :]).astype(
        jnp.bfloat16
    )
    chooser = jnp.sum(chooser.reshape(rows, top_count, experts * capacity), axis=1)
    outgoing = jnp.einsum("rs,rc->sc", chooser, normed, preferred_element_type=jnp.float32).astype(
        jnp.bfloat16
    )
    outgoing = outgoing.reshape(n_sp, local_experts, capacity, normed.shape[1])
    arrived = lax.all_to_all(outgoing, "sp", split_axis=0, concat_axis=0, tiled=True)
    gate_part = jnp.einsum("segd,edf->segf", arrived, exp_gate, preferred_element_type=jnp.float32)
    up_part = jnp.einsum("segd,edf->segf", arrived, exp_up, preferred_element_type=jnp.float32)
    gate_pre = lax.psum(gate_part.astype(jnp.bfloat16), TP).astype(jnp.float32)
    up_pre = lax.psum(up_part.astype(jnp.bfloat16), TP).astype(jnp.float32)
    hidden = (jax.nn.silu(gate_pre) * up_pre).astype(jnp.bfloat16)
    produced = jnp.einsum("segf,efd->segd", hidden, exp_down, preferred_element_type=jnp.float32)
    returned = lax.all_to_all(
        produced.astype(jnp.bfloat16), "sp", split_axis=0, concat_axis=0, tiled=True
    )
    flat_back = returned.reshape(experts * capacity, returned.shape[3])
    picked = jnp.take(flat_back, slot, axis=0).reshape(rows, top_count, returned.shape[3])
    routed = jnp.sum(gates[:, :, None] * picked.astype(jnp.float32), axis=1)
    moe = routed + shared_out
    result = stream_f + moe
    return result.astype(jnp.bfloat16)


def solution(mesh):
    finer = Mesh(mesh.devices.reshape(mesh.shape["sp"], 4, 4), ("sp", "tp_0", "tp_1"))
    in_specs = (
        P("sp", TP),
        P("sp", TP),
        P("sp", TP),
        P("sp", TP),
        P("sp", TP),
        P("sp", TP),
        P("sp", TP),
        P("sp", TP),
        P(TP, None),
        P(TP, None),
        P("sp", TP),
        P(TP),
        P(TP),
        P("sp", None),
        P("sp", None),
        P("sp", TP, None),
        P("sp", TP, None),
        P("sp", None, TP),
        P(TP, None),
        P(TP, None),
        P(None, TP),
    )
    out_specs = P("sp", TP)
    return jax.shard_map(
        shards, mesh=finer, in_specs=in_specs, out_specs=out_specs, check_vma=False
    )
```

profile of v0, /device:TPU:1, one launch (start us, length us, event | category | flops | bytes accessed | tf_op | source)
XLA Modules:
  0.0 487.4 jit_solution(6028487693172046048)
XLA Ops:
  6.5 1.6 pad_maximum_fusion
  8.2 0.9 copy.128
  9.1 0.9 copy.131
  10.0 0.9 copy.127
  10.9 0.8 copy.137
  11.7 0.1 eq.40
  11.9 0.1 copy.139
  12.0 1.1 fusion.127
  13.2 0.5 fusion.75
  13.7 0.3 fusion.133
  14.0 0.3 fusion.98
  14.3 0.2 fusion.99
  14.5 0.8 fusion.73
  15.3 76.1 %all-gather.2.cloned.1.call-done = bf16[6144,512]{1,0:T(8,128)(2,1)} async-done(((bf16[192,512]{1,0:T(8,128)(2,1)}), bf16[6144,512]{1,0:T(8,128)(2,1)}) %all-gather.2.cloned.1.call-update) | async-done | bytes 6291472 | tf_op jit(solution)/shard_map/all_gather | solution.py:138
  91.4 8.7 %copy.134 = bf16[6144,512]{0,1:T(8,128)(2,1)} copy(bf16[6144,512]{1,0:T(8,128)(2,1)} %all-gather.2.cloned.1.call-done) | data formatting | bytes 12582912 | tf_op jit(solution)/shard_map/while | solution.py:150
  100.1 6.4 %while.19 = (s32[]{:T(128)}, f32[192,2,64]{0,2,1:T(8,128)S(1)}, f32[192,1,128]{2,0,1:T(8,128)S(1)}, f32[2,192]{1,0:T(2,128)S(1)}, f32[1,192]{1,0:T(1,128)S(1)}, ...) while((s32[]{:T(128)}, f32[192,2,64]{0,2,1:T(8,128)S(1)}, ...), condition=%wide.region_7.8_spmd, body=%wide.region_2.7_spmd.sunk | while | flops 83325512 | bytes 2064037 | solution.py:150
  100.1 5.1 %conditional.2 = ((f32[192,2,64]{0,2,1:T(8,128)S(1)}, f32[192,1,128]{2,0,1:T(8,128)S(1)}, f32[2,192]{1,0:T(2,128)S(1)}, f32[1,192]{1,0:T(1,128)S(1)})) conditional(s32[]{:T(128)} %convert_element_type.258, (f32[192,2,64]{0,2,1:T(8,128)S(1)}, f32[192,1,128]{2,0,1:T(8,128)S(1)}, f32[2,192]{1,0:T(2,128)S(1)}, f32[1,192]{1,0:T(1,128)S(1)}) %tuple.58, ...), branch_computations={%region_3.3_spmd, %region_4.6_spmd} | conditional | flops 83325512 | bytes 2063786 | solution.py:143
  100.1 1.1 constant_dynamic-slice_fusion
  101.1 0.5 fusion.25
  101.6 0.7 fusion.12
  102.4 1.3 fusion.43
  103.7 1.5 fusion.13
  106.5 0.4 fusion.154
  106.9 0.6 copy-done.1
  107.5 0.4 fusion.60
  107.9 1.1 copy.166
  109.0 6.7 %all-to-all-start = ((bf16[16,192,128]{2,1,0:T(8,128)(2,1)}), bf16[16,192,128]{2,1,0:T(8,128)(2,1)S(1)}, u32[]{:S(2)}, u32[]{:S(2)}) async-start(bf16[16,192,128]{2,1,0:T(8,128)(2,1)} %bitcast.107), calls=%async_computation | async-start | bytes 1572864 | tf_op jit(solution)/shard_map/all_to_all | solution.py:19
  115.7 0.1 reshape.279
  116.0 0.2 fusion.108
  116.2 0.1 reduce_sum.108
  116.4 0.1 copy.141
  116.5 0.2 fusion.83
  116.6 9.7 %all-to-all-done = bf16[16,192,128]{2,1,0:T(8,128)(2,1)S(1)} async-done(((bf16[16,192,128]{2,1,0:T(8,128)(2,1)}), bf16[16,192,128]{2,1,0:T(8,128)(2,1)S(1)}, u32[]{:S(2)}, u32[]{:S(2)}) %all-to-all-start) | async-done | bytes 786464 | tf_op jit(solution)/shard_map/all_to_all | solution.py:19
  126.3 0.1 convert_reduce_fusion
  126.5 0.1 multiply_reduce_fusion.1
  126.6 6.5 %psum.56 = f32[192]{0:T(256)S(1)} all-reduce(f32[192]{0:T(256)S(1)} %multiply_reduce_fusion.1), channel_id=1, replica_groups=mesh['sp'=32,'tp_0'=4,'tp_1'=4] {'tp_0'}, use_global_device_ids=true, to_apply=%region_10.11 | all-reduce | flops 192 | bytes 1536 | tf_op jit(solution)/shard_map/psum | solution.py:25
  133.1 6.8 %psum.57 = f32[192]{0:T(256)S(1)} all-reduce(f32[192]{0:T(256)S(1)} %psum.56), channel_id=1, replica_groups=mesh['sp'=32,'tp_0'=4,'tp_1'=4] {'tp_1'}, use_global_device_ids=true, to_apply=%region_11.12 | all-reduce | flops 192 | bytes 1536 | tf_op jit(solution)/shard_map/psum | solution.py:25
  139.9 0.1 add_convert_fusion
  140.0 0.1 fusion.130
  140.1 6.5 %psum.58 = f32[192]{0:T(256)S(1)} all-reduce(f32[192]{0:T(256)S(1)} %fusion.130), channel_id=1, replica_groups=mesh['sp'=32,'tp_0'=4,'tp_1'=4] {'tp_0'}, use_global_device_ids=true, to_apply=%region_17.18 | all-reduce | flops 192 | bytes 1536 | tf_op jit(solution)/shard_map/psum | solution.py:25
  146.6 7.1 %psum.59 = f32[192]{0:T(256)S(1)} all-reduce(f32[192]{0:T(256)S(1)} %psum.58), channel_id=1, replica_groups=mesh['sp'=32,'tp_0'=4,'tp_1'=4] {'tp_1'}, use_global_device_ids=true, to_apply=%region_18.19 | all-reduce | flops 192 | bytes 1536 | tf_op jit(solution)/shard_map/psum | solution.py:25
  153.7 0.3 convolution_convert_fusion.5
  154.1 0.1 reshape.281
  154.1 0.7 copy.143
  154.9 161.9 %all-to-all-start.1 = ((bf16[32,4,5,128]{3,1,2,0:T(4,128)(2,1)}), bf16[32,4,5,128]{3,1,2,0:T(4,128)(2,1)S(1)}, u32[]{:S(2)}, u32[]{:S(2)}) async-start(bf16[32,4,5,128]{3,1,2,0:T(4,128)(2,1)} %copy.143), calls=%async_computation.1 | async-start | bytes 327680 | tf_op jit(solution)/shard_map/all_to_all | solution.py:193
  316.8 0.9 convolution_convert_fusion.3
  317.7 0.9 convolution_convert_fusion.2
  318.7 15.2 %all-to-all-done.1 = bf16[32,4,5,128]{3,1,2,0:T(4,128)(2,1)S(1)} async-done(((bf16[32,4,5,128]{3,1,2,0:T(4,128)(2,1)}), bf16[32,4,5,128]{3,1,2,0:T(4,128)(2,1)S(1)}, u32[]{:S(2)}, u32[]{:S(2)}) %all-to-all-start.1) | async-done | bytes 163872 | tf_op jit(solution)/shard_map/all_to_all | solution.py:193
  333.9 1.2 fusion.61
  335.0 1.2 fusion.62
  336.2 106.3 %all-reduce.3.cloned.1.call-done = (bf16[32,4,5,512]{3,0,2,1:T(8,128)(2,1)}, bf16[32,4,5,512]{3,0,2,1:T(8,128)(2,1)}, bf16[192,512]{1,0:T(8,128)(2,1)}, bf16[192,512]{1,0:T(8,128)(2,1)}) async-done(((bf16[32,4,5,512]{3,0,2,1:T(8,128)(2,1)}, bf16[32,4,5,512]{3,0,2,1:T(8,128)(2,1)}, bf16[192,512]{1,0:T(8,128)(2,1)}, bf16[192,512]{1,0:T(8,128)(2,1)}), (bf16[32,4,5,512]{3,0,2,1:T(8,128)(2,1)}, ...) | async-done | bytes 1703952 | tf_op jit(solution)/shard_map/psum | solution.py:197
  442.6 1.8 fusion.71
  444.5 0.7 copy.146
  445.2 14.6 %all-to-all-start.2 = ((bf16[32,4,5,128]{3,1,2,0:T(4,128)(2,1)}), bf16[32,4,5,128]{3,1,2,0:T(4,128)(2,1)S(1)}, u32[]{:S(2)}, u32[]{:S(2)}) async-start(bf16[32,4,5,128]{3,1,2,0:T(4,128)(2,1)} %copy.146), calls=%async_computation.2 | async-start | bytes 327680 | tf_op jit(solution)/shard_map/all_to_all | solution.py:200
  459.8 0.1 copy.148
  460.0 0.1 mul.135
  460.1 0.2 copy.142
  460.3 0.1 copy.136
  460.5 16.5 %all-to-all-done.2 = bf16[32,4,5,128]{3,1,2,0:T(4,128)(2,1)S(1)} async-done(((bf16[32,4,5,128]{3,1,2,0:T(4,128)(2,1)}), bf16[32,4,5,128]{3,1,2,0:T(4,128)(2,1)S(1)}, u32[]{:S(2)}, u32[]{:S(2)}) %all-to-all-start.2) | async-done | bytes 163872 | tf_op jit(solution)/shard_map/all_to_all | solution.py:200
  477.0 0.1 copy.147
  477.0 0.1 reshape.282
  477.1 1.4 gather_fusion
  478.6 1.1 multiply_reduce_fusion
  479.7 0.9 fusion.77
  (86 shorter events, 0.8 us)
Async XLA Ops:
  6.5 100.0 %copy-start = (bf16[128,2048]{1,0:T(8,128)(2,1)S(1)}, bf16[128,2048]{1,0:T(8,128)(2,1)}, u32[]{:S(2)}) copy-start(bf16[128,2048]{1,0:T(8,128)(2,1)} %param.33) | copy-start | bytes 1572868
  6.5 6.6 %copy-start.6 = (bf16[192,128]{1,0:T(8,128)(2,1)S(1)}, bf16[192,128]{1,0:T(8,128)(2,1)}, u32[]{:S(2)}) copy-start(bf16[192,128]{1,0:T(8,128)(2,1)} %param.30) | copy-start | bytes 147460
  6.5 84.8 %all-gather.2.cloned.1.call-start = ((), (), s32[]{:S(2)}) async-start(), calls=%async_computation.3 | async-start | bytes 6488064 | tf_op jit(solution)/shard_map/all_gather | solution.py:138
  8.2 5.5 %copy-start.10 = (f32[192,2]{0,1:T(2,128)S(1)}, f32[192,2]{0,1:T(2,128)}, u32[]{:S(2)}) copy-start(f32[192,2]{0,1:T(2,128)} %param.31) | copy-start | bytes 4612
  15.2 84.8 %copy-start.17 = (bf16[192,128]{1,0:T(8,128)(2,1)S(1)}, bf16[192,128]{1,0:T(8,128)(2,1)}, u32[]{:S(2)}) copy-start(bf16[192,128]{1,0:T(8,128)(2,1)} %param.28) | copy-start | bytes 147460
  15.3 84.8 %copy-start.18 = (f32[192,1]{0,1:T(1,128)S(1)}, f32[192,1]{0,1:T(1,128)}, u32[]{:S(2)}) copy-start(f32[192,1]{0,1:T(1,128)} %param.32) | copy-start | bytes 2308
  106.5 1.0 copy-start.1
  109.0 7.4 %copy-start.8 = (s32[192,2]{0,1:T(2,128)S(1)}, s32[192,2]{0,1:T(2,128)}, u32[]{:S(2)}) copy-start(s32[192,2]{0,1:T(2,128)} %param.38) | copy-start | bytes 4612
  109.0 17.3 %all-to-all-start = ((bf16[16,192,128]{2,1,0:T(8,128)(2,1)}), bf16[16,192,128]{2,1,0:T(8,128)(2,1)S(1)}, u32[]{:S(2)}, u32[]{:S(2)}) async-start(bf16[16,192,128]{2,1,0:T(8,128)(2,1)} %bitcast.107), calls=%async_computation | async-start | bytes 1572864 | tf_op jit(solution)/shard_map/all_to_all | solution.py:19
  115.7 24.2 %copy-start.7 = (bf16[192,128]{1,0:T(8,128)(2,1)S(1)}, bf16[192,128]{1,0:T(8,128)(2,1)}, u32[]{:S(2)}) copy-start(bf16[192,128]{1,0:T(8,128)(2,1)} %param.35) | copy-start | bytes 147460
  115.7 24.2 %copy-start.12 = (f32[128]{0:T(128)S(1)}, f32[128]{0:T(128)}, u32[]{:S(2)}) copy-start(f32[128]{0:T(128)} %param.36) | copy-start | bytes 1540
  115.7 38.0 %copy-start.9 = (f32[128]{0:T(128)S(1)}, f32[128]{0:T(128)}, u32[]{:S(2)}) copy-start(f32[128]{0:T(128)} %param.37) | copy-start | bytes 1540
  116.4 200.3 %copy-start.4 = (bf16[128,512]{1,0:T(8,128)(2,1)S(1)}, bf16[128,512]{1,0:T(8,128)(2,1)}, u32[]{:S(2)}) copy-start(bf16[128,512]{1,0:T(8,128)(2,1)} %param.43) | copy-start | bytes 393220
  116.6 201.1 %copy-start.5 = (bf16[128,512]{1,0:T(8,128)(2,1)S(1)}, bf16[128,512]{1,0:T(8,128)(2,1)}, u32[]{:S(2)}) copy-start(bf16[128,512]{1,0:T(8,128)(2,1)} %param.44) | copy-start | bytes 393220
  126.4 207.4 %copy-start.2 = (bf16[4,128,512]{2,1,0:T(8,128)(2,1)S(1)}, bf16[4,128,512]{2,1,0:T(8,128)(2,1)}, u32[]{:S(2)}) copy-start(bf16[4,128,512]{2,1,0:T(8,128)(2,1)} %param.40) | copy-start | bytes 1572868
  154.0 181.0 %copy-start.3 = (bf16[4,128,512]{2,1,0:T(8,128)(2,1)S(1)}, bf16[4,128,512]{2,1,0:T(8,128)(2,1)}, u32[]{:S(2)}) copy-start(bf16[4,128,512]{2,1,0:T(8,128)(2,1)} %param.41) | copy-start | bytes 1572868
  154.9 179.0 %all-to-all-start.1 = ((bf16[32,4,5,128]{3,1,2,0:T(4,128)(2,1)}), bf16[32,4,5,128]{3,1,2,0:T(4,128)(2,1)S(1)}, u32[]{:S(2)}, u32[]{:S(2)}) async-start(bf16[32,4,5,128]{3,1,2,0:T(4,128)(2,1)} %copy.143), calls=%async_computation.1 | async-start | bytes 327680 | tf_op jit(solution)/shard_map/all_to_all | solution.py:193
  316.7 125.9 %all-reduce.3.cloned.1.call-start = ((), (), s32[]{:S(2)}) async-start(), calls=%async_computation.4 | async-start | bytes 3407872 | tf_op jit(solution)/shard_map/psum | solution.py:197
  335.0 107.6 %copy-start.13 = (bf16[4,512,128]{2,1,0:T(8,128)(2,1)S(1)}, bf16[4,512,128]{2,1,0:T(8,128)(2,1)}, u32[]{:S(2)}) copy-start(bf16[4,512,128]{2,1,0:T(8,128)(2,1)} %param.42) | copy-start | bytes 1572868
  442.6 17.7 %copy-start.11 = (f32[192,2]{0,1:T(2,128)S(1)}, f32[192,2]{0,1:T(2,128)}, u32[]{:S(2)}) copy-start(f32[192,2]{0,1:T(2,128)} %param.39) | copy-start | bytes 4612
  444.4 35.2 %copy-start.14 = (bf16[192,512]{1,0:T(8,128)(2,1)S(1)}, bf16[192,512]{1,0:T(8,128)(2,1)}, u32[]{:S(2)}) copy-start(bf16[192,512]{1,0:T(8,128)(2,1)} %get-tuple-element.401) | copy-start | bytes 589828
  444.5 35.2 %copy-start.15 = (bf16[192,512]{1,0:T(8,128)(2,1)S(1)}, bf16[192,512]{1,0:T(8,128)(2,1)}, u32[]{:S(2)}) copy-start(bf16[192,512]{1,0:T(8,128)(2,1)} %get-tuple-element.402) | copy-start | bytes 589828
  444.5 35.2 %copy-start.16 = (bf16[512,128]{1,0:T(8,128)(2,1)S(1)}, bf16[512,128]{1,0:T(8,128)(2,1)}, u32[]{:S(2)}) copy-start(bf16[512,128]{1,0:T(8,128)(2,1)} %param.45) | copy-start | bytes 393220
  445.2 31.7 %all-to-all-start.2 = ((bf16[32,4,5,128]{3,1,2,0:T(4,128)(2,1)}), bf16[32,4,5,128]{3,1,2,0:T(4,128)(2,1)S(1)}, u32[]{:S(2)}, u32[]{:S(2)}) async-start(bf16[32,4,5,128]{3,1,2,0:T(4,128)(2,1)} %copy.146), calls=%async_computation.2 | async-start | bytes 327680 | tf_op jit(solution)/shard_map/all_to_all | solution.py:200
Sparse Core Ops, SparseCore 0:
  9.5 81.8 all-gather.1
  336.4 106.1 all-reduce.2
where the time goes:
time: 491 us; the launch traced here: 487 us
  waiting for transfers between devices  224 us (46%)
  starting transfers between devices  183 us (37%)
  blocking collectives  26.9 us (5%)
  local copies, waits for them, and re-layouts  19.3 us (4%)
  matrix products  14.7 us (3%)
  between operations  13.9 us (3%)
    all_to_all x1, starting transfers between devices, shards(): lax.all_to_all(outgoing, 'sp', split_axis=0, concat_axis=0, tiled=True)  162 us
    psum x1, waiting for transfers between devices, shards(): up_pre = lax.psum(up_part.astype(jnp.bfloat16), TP).astype(jnp.float32)  106 us
    all_gather x1, waiting for transfers between devices, shards(): gathered = lax.all_gather(joined_local, 'sp', axis=0, tiled=True)  76.1 us
    psum x4, blocking collectives, by_axis(): x = lax.psum(x, axis)  26.9 us
    all_to_all x1, waiting for transfers between devices, shards(): lax.all_to_all(produced.astype(jnp.bfloat16), 'sp', split_axis=0, concat_...  16.5 us
    all_to_all x1, waiting for transfers between devices, shards(): lax.all_to_all(outgoing, 'sp', split_axis=0, concat_axis=0, tiled=True)  15.2 us
    all_to_all x1, starting transfers between devices, shards(): lax.all_to_all(produced.astype(jnp.bfloat16), 'sp', split_axis=0, concat_...  14.6 us
  transfers between devices with their start and end apart: 5, of which 5 were waited for; matrix products, arithmetic and copies ran while one was open for 2% of the time, Pallas kernels for 0%

commit v1 on v0

--- a/solution.py
+++ b/solution.py
@@ -3,6 +3,7 @@
 from jax import lax
 from jax.sharding import Mesh
 from jax.sharding import PartitionSpec as P
+from jax.lax import axis_index, axis_size, ppermute
 
 D = 2048
 TP = ("tp_0", "tp_1")
@@ -135,7 +136,16 @@
     state = stick_block(
         empty_state(rows, heads_a, size_a, heads_b, size_b), queries, unpack(joined_local), causal
     )
-    gathered = lax.all_gather(joined_local, "sp", axis=0, tiled=True)
+    back = axis_index("sp")
+    z1 = axis_size("sp")
+    f_now, v1 = (z1, back)
+    gathered, out_arr = (joined_local, 1)
+    while out_arr < f_now:
+        block_next = ppermute(gathered, "sp", [(t, t ^ out_arr) for t in range(f_now)])
+        t_next = jnp.concatenate([gathered, block_next], axis=0)
+        carry_in = jnp.concatenate([block_next, gathered], 0)
+        gathered = jnp.where(v1 & out_arr == 0, t_next, carry_in)
+        out_arr = 2 * out_arr
 
     def turn(step, inner_state):
         start = jnp.maximum(position - step, 0) * rows

time: 491 us -> 913 us (1.86)
  waiting for transfers between devices: 224 us -> 525 us
  starting transfers between devices: 183 us -> 300 us
  other arithmetic: 4.28 us -> 17.5 us
    ppermute x0 -> x5, waiting for transfers between devices: none -> 377 us  [shards(): ppermute(gathered, 'sp', [(t, t ^ out_arr) for t in range(f_now)])]
    all_to_all x1, starting transfers between devices: 6.67 us -> 152 us  [sum_at_owner(): lax.all_to_all(tiles, axis, split_axis=0, concat_axis=0, tiled=True)]
    all_gather x1 -> x0, waiting for transfers between devices: 76.1 us -> none  [shards(): gathered = lax.all_gather(joined_local, 'sp', axis=0, tiled=True)]
    all_to_all x1, starting transfers between devices: 162 us -> 106 us  [shards(): lax.all_to_all(outgoing, 'sp', split_axis=0, concat_axis=0, tiled=True)]
    ppermute x0 -> x5, starting transfers between devices: none -> 26.9 us  [shards(): ppermute(gathered, 'sp', [(t, t ^ out_arr) for t in range(f_now)])]
    select_n x0 -> x5, other arithmetic: none -> 14.8 us  [shards(): gathered = jnp.where(v1 & out_arr == 0, t_next, carry_in)]
  transfers between devices with their start and end apart: 5 -> 9, of which waited for: 5 -> 9; matrix products, arithmetic and copies ran while one was open for 2% -> 1% of each run, Pallas kernels for 0% -> 0%
where the time goes in v1:
time: 913 us; the launch traced here: 909 us
  waiting for transfers between devices  525 us (58%)
  starting transfers between devices  300 us (33%)
  blocking collectives  26.9 us (3%)
  other arithmetic  17.5 us (2%)
  between operations  14 us (2%)
  matrix products  13.9 us (2%)
  local copies, waits for them, and re-layouts  10.4 us (1%)
    ppermute x5, waiting for transfers between devices, shards(): ppermute(gathered, 'sp', [(t, t ^ out_arr) for t in range(f_now)])  377 us
    all_to_all x1, starting transfers between devices, sum_at_owner(): lax.all_to_all(tiles, axis, split_axis=0, concat_axis=0, tiled=True)  152 us
    all_to_all x1, starting transfers between devices, shards(): lax.all_to_all(outgoing, 'sp', split_axis=0, concat_axis=0, tiled=True)  106 us
    psum x1, waiting for transfers between devices, shards(): up_pre = lax.psum(up_part.astype(jnp.bfloat16), TP).astype(jnp.float32)  106 us
    ppermute x5, starting transfers between devices, shards(): ppermute(gathered, 'sp', [(t, t ^ out_arr) for t in range(f_now)])  26.9 us
    psum x4, blocking collectives, by_axis(): x = lax.psum(x, axis)  26.9 us
  transfers between devices with their start and end apart: 9, of which 9 were waited for; matrix products, arithmetic and copies ran while one was open for 1% of the time, Pallas kernels for 0%

profile of v1, /device:TPU:1, one launch (start us, length us, event | category | flops | bytes accessed | tf_op | source)
XLA Modules:
  0.0 909.3 jit_solution(2390480599174362944)
XLA Ops:
  6.5 1.0 copy.137
  7.5 0.9 copy.140
  8.4 0.9 copy.145
  9.3 0.9 copy.146
  10.3 8.7 collective-permute-start
  19.0 1.1 collective-permute-done
  20.2 0.3 maximum_select_fusion.4
  20.5 1.9 collective-permute-start.1
  22.4 10.3 %collective-permute-done.1 = bf16[384,512]{0,1:T(8,128)(2,1)S(1)} collective-permute-done((bf16[384,512]{0,1:T(8,128)(2,1)S(1)}, bf16[384,512]{0,1:T(8,128)(2,1)S(1)}, u32[]{:S(2)}, u32[]{:S(2)}) %collective-permute-start.1) | collective-permute-done | bytes 393248 | tf_op jit(solution)/shard_map/ppermute | solution.py:144
  32.6 0.2 maximum_select_fusion.3
  32.8 1.9 collective-permute-start.2
  34.8 37.3 %collective-permute-done.2 = bf16[768,512]{0,1:T(8,128)(2,1)} collective-permute-done((bf16[768,512]{0,1:T(8,128)(2,1)S(1)}, bf16[768,512]{0,1:T(8,128)(2,1)}, u32[]{:S(2)}, u32[]{:S(2)}) %collective-permute-start.2) | collective-permute-done | bytes 786464 | tf_op jit(solution)/shard_map/ppermute | solution.py:144
  72.0 1.7 maximum_select_fusion.2
  73.8 3.5 collective-permute-start.3
  77.4 204.9 %collective-permute-done.3 = bf16[1536,512]{0,1:T(8,128)(2,1)} collective-permute-done((bf16[1536,512]{0,1:T(8,128)(2,1)S(1)}, bf16[1536,512]{0,1:T(8,128)(2,1)}, u32[]{:S(2)}, u32[]{:S(2)}) %collective-permute-start.3) | collective-permute-done | bytes 1572896 | tf_op jit(solution)/shard_map/ppermute | solution.py:144
  282.2 4.0 maximum_select_fusion.1
  286.2 10.8 %collective-permute-start.4 = (bf16[3072,512]{0,1:T(8,128)(2,1)}, bf16[3072,512]{0,1:T(8,128)(2,1)}, u32[]{:S(2)}, u32[]{:S(2)}) collective-permute-start(bf16[3072,512]{0,1:T(8,128)(2,1)} %maximum_select_fusion.1), channel_id=1, source_target_pairs={{0,256},{16,272},{32,288},{48,304},{64,320},{80,336},{96,352},{112... | collective-permute-start | bytes 9437192 | tf_op jit(solution)/shard_map/ppermute | solution.py:144
  297.3 0.1 eq.60
  297.6 0.3 fusion.127
  298.0 0.5 fusion.75
  298.5 0.3 fusion.133
  298.8 0.3 fusion.98
  299.1 0.2 fusion.99
  299.3 0.8 fusion.73
  300.0 123.1 %collective-permute-done.4 = bf16[3072,512]{0,1:T(8,128)(2,1)} collective-permute-done((bf16[3072,512]{0,1:T(8,128)(2,1)}, bf16[3072,512]{0,1:T(8,128)(2,1)}, u32[]{:S(2)}, u32[]{:S(2)}) %collective-permute-start.4) | collective-permute-done | bytes 3145760 | tf_op jit(solution)/shard_map/ppermute | solution.py:144
  423.2 8.6 maximum_select_fusion
  431.8 6.5 while.19
  431.8 5.1 conditional.2
  431.8 1.1 constant_dynamic-slice_fusion
  432.9 0.5 fusion.25
  433.4 0.7 fusion.12
  434.1 1.3 fusion.43
  435.4 1.5 fusion.13
  438.3 0.4 fusion.154
  438.7 0.4 fusion.60
  439.1 1.1 copy.178
  440.2 151.7 %all-to-all-start = ((bf16[16,192,128]{2,1,0:T(8,128)(2,1)}), bf16[16,192,128]{2,1,0:T(8,128)(2,1)S(1)}, u32[]{:S(2)}, u32[]{:S(2)}) async-start(bf16[16,192,128]{2,1,0:T(8,128)(2,1)} %bitcast.107), calls=%async_computation | async-start | bytes 1572864 | tf_op jit(solution)/shard_map/all_to_all | solution.py:20
  591.9 0.1 reshape.279
  592.2 0.2 fusion.108
  592.4 0.1 reduce_sum.108
  592.7 0.2 fusion.83
  592.9 10.6 %all-to-all-done = bf16[16,192,128]{2,1,0:T(8,128)(2,1)S(1)} async-done(((bf16[16,192,128]{2,1,0:T(8,128)(2,1)}), bf16[16,192,128]{2,1,0:T(8,128)(2,1)S(1)}, u32[]{:S(2)}, u32[]{:S(2)}) %all-to-all-start) | async-done | bytes 786464 | tf_op jit(solution)/shard_map/all_to_all | solution.py:20
  603.7 6.5 psum.56
  610.2 6.6 psum.57
  617.1 6.6 psum.58
  623.7 7.1 psum.59
  630.8 0.3 convolution_convert_fusion.5
  631.3 0.7 copy.155
  632.0 106.5 %all-to-all-start.1 = ((bf16[32,4,5,128]{3,1,2,0:T(4,128)(2,1)}), bf16[32,4,5,128]{3,1,2,0:T(4,128)(2,1)S(1)}, u32[]{:S(2)}, u32[]{:S(2)}) async-start(bf16[32,4,5,128]{3,1,2,0:T(4,128)(2,1)} %copy.155), calls=%async_computation.1 | async-start | bytes 327680 | tf_op jit(solution)/shard_map/all_to_all | solution.py:203
  738.5 0.9 convolution_convert_fusion.3
  739.5 0.9 convolution_convert_fusion.2
  740.4 15.2 %all-to-all-done.1 = bf16[32,4,5,128]{3,1,2,0:T(4,128)(2,1)S(1)} async-done(((bf16[32,4,5,128]{3,1,2,0:T(4,128)(2,1)}), bf16[32,4,5,128]{3,1,2,0:T(4,128)(2,1)S(1)}, u32[]{:S(2)}, u32[]{:S(2)}) %all-to-all-start.1) | async-done | bytes 163872 | tf_op jit(solution)/shard_map/all_to_all | solution.py:203
  755.6 1.2 fusion.61
  756.8 1.2 fusion.62
  758.0 106.4 %all-reduce.3.cloned.1.call-done = (bf16[32,4,5,512]{3,0,2,1:T(8,128)(2,1)}, bf16[32,4,5,512]{3,0,2,1:T(8,128)(2,1)}, bf16[192,512]{1,0:T(8,128)(2,1)}, bf16[192,512]{1,0:T(8,128)(2,1)}) async-done(((bf16[32,4,5,512]{3,0,2,1:T(8,128)(2,1)}, bf16[32,4,5,512]{3,0,2,1:T(8,128)(2,1)}, bf16[192,512]{1,0:T(8,128)(2,1)}, bf16[192,512]{1,0:T(8,128)(2,1)}), (bf16[32,4,5,512]{3,0,2,1:T(8,128)(2,1)}, ...) | async-done | bytes 1703952 | tf_op jit(solution)/shard_map/psum | solution.py:207
  864.4 1.9 fusion.71
  866.3 0.7 copy.158
  867.1 14.6 %all-to-all-start.2 = ((bf16[32,4,5,128]{3,1,2,0:T(4,128)(2,1)}), bf16[32,4,5,128]{3,1,2,0:T(4,128)(2,1)S(1)}, u32[]{:S(2)}, u32[]{:S(2)}) async-start(bf16[32,4,5,128]{3,1,2,0:T(4,128)(2,1)} %copy.158), calls=%async_computation.2 | async-start | bytes 327680 | tf_op jit(solution)/shard_map/all_to_all | solution.py:210
  881.8 0.1 mul.135
  882.0 0.2 copy.154
  882.3 16.5 %all-to-all-done.2 = bf16[32,4,5,128]{3,1,2,0:T(4,128)(2,1)S(1)} async-done(((bf16[32,4,5,128]{3,1,2,0:T(4,128)(2,1)}), bf16[32,4,5,128]{3,1,2,0:T(4,128)(2,1)S(1)}, u32[]{:S(2)}, u32[]{:S(2)}) %all-to-all-start.2) | async-done | bytes 163872 | tf_op jit(solution)/shard_map/all_to_all | solution.py:210
  898.9 1.4 gather_fusion
  900.4 1.1 multiply_reduce_fusion
  901.5 0.9 fusion.77
  (103 shorter events, 2.1 us)
Async XLA Ops:
  6.5 431.8 %copy-start = (bf16[128,2048]{1,0:T(8,128)(2,1)S(1)}, bf16[128,2048]{1,0:T(8,128)(2,1)}, u32[]{:S(2)}) copy-start(bf16[128,2048]{1,0:T(8,128)(2,1)} %param.33) | copy-start | bytes 1572868
  10.3 9.9 %collective-permute-start = (bf16[192,512]{0,1:T(8,128)(2,1)S(1)}, bf16[192,512]{0,1:T(8,128)(2,1)S(1)}, u32[]{:S(2)}, u32[]{:S(2)}) collective-permute-start(bf16[192,512]{0,1:T(8,128)(2,1)S(1)} %pad_maximum_fusion), channel_id=1, source_target_pairs={{0,16},{16,0},{32,48},{48,32},{64,80},{80,64},{96,112},{112,96},{1... | collective-permute-start | bytes 589832 | tf_op jit(solution)/shard_map/ppermute | solution.py:144
  20.5 12.2 %collective-permute-start.1 = (bf16[384,512]{0,1:T(8,128)(2,1)S(1)}, bf16[384,512]{0,1:T(8,128)(2,1)S(1)}, u32[]{:S(2)}, u32[]{:S(2)}) collective-permute-start(bf16[384,512]{0,1:T(8,128)(2,1)S(1)} %maximum_select_fusion.4), channel_id=1, source_target_pairs={{0,32},{16,48},{32,0},{48,16},{64,96},{80,112},{96,64},{112,80},{1... | collective-permute-start | bytes 1179656 | tf_op jit(solution)/shard_map/ppermute | solution.py:144
  32.8 39.2 %collective-permute-start.2 = (bf16[768,512]{0,1:T(8,128)(2,1)S(1)}, bf16[768,512]{0,1:T(8,128)(2,1)}, u32[]{:S(2)}, u32[]{:S(2)}) collective-permute-start(bf16[768,512]{0,1:T(8,128)(2,1)S(1)} %maximum_select_fusion.3), channel_id=1, source_target_pairs={{0,64},{16,80},{32,96},{48,112},{64,0},{80,16},{96,32},{112,48},{1... | collective-permute-start | bytes 2359304 | tf_op jit(solution)/shard_map/ppermute | solution.py:144
  73.8 208.5 %collective-permute-start.3 = (bf16[1536,512]{0,1:T(8,128)(2,1)S(1)}, bf16[1536,512]{0,1:T(8,128)(2,1)}, u32[]{:S(2)}, u32[]{:S(2)}) collective-permute-start(bf16[1536,512]{0,1:T(8,128)(2,1)S(1)} %maximum_select_fusion.2), channel_id=1, source_target_pairs={{0,128},{16,144},{32,160},{48,176},{64,192},{80,208},{96,224},{112... | collective-permute-start | bytes 4718600 | tf_op jit(solution)/shard_map/ppermute | solution.py:144
  77.3 219.8 %copy-start.6 = (bf16[192,128]{1,0:T(8,128)(2,1)S(1)}, bf16[192,128]{1,0:T(8,128)(2,1)}, u32[]{:S(2)}) copy-start(bf16[192,128]{1,0:T(8,128)(2,1)} %param.25) | copy-start | bytes 147460
  77.3 219.9 %copy-start.10 = (s32[192,2]{0,1:T(2,128)S(1)}, s32[192,2]{0,1:T(2,128)}, u32[]{:S(2)}) copy-start(s32[192,2]{0,1:T(2,128)} %param.38) | copy-start | bytes 4612
  77.3 220.3 %copy-start.7 = (bf16[192,128]{1,0:T(8,128)(2,1)S(1)}, bf16[192,128]{1,0:T(8,128)(2,1)}, u32[]{:S(2)}) copy-start(bf16[192,128]{1,0:T(8,128)(2,1)} %param.29) | copy-start | bytes 147460
  77.3 220.3 %copy-start.19 = (bf16[192,128]{1,0:T(8,128)(2,1)S(1)}, bf16[192,128]{1,0:T(8,128)(2,1)}, u32[]{:S(2)}) copy-start(bf16[192,128]{1,0:T(8,128)(2,1)} %param.28) | copy-start | bytes 147460
  77.3 220.3 %copy-start.20 = (f32[192,1]{0,1:T(1,128)S(1)}, f32[192,1]{0,1:T(1,128)}, u32[]{:S(2)}) copy-start(f32[192,1]{0,1:T(1,128)} %param.32) | copy-start | bytes 2308
  77.3 220.6 %copy-start.8 = (bf16[192,128]{1,0:T(8,128)(2,1)S(1)}, bf16[192,128]{1,0:T(8,128)(2,1)}, u32[]{:S(2)}) copy-start(bf16[192,128]{1,0:T(8,128)(2,1)} %param.30) | copy-start | bytes 147460
  77.4 221.1 %copy-start.12 = (f32[192,2]{0,1:T(2,128)S(1)}, f32[192,2]{0,1:T(2,128)}, u32[]{:S(2)}) copy-start(f32[192,2]{0,1:T(2,128)} %param.31) | copy-start | bytes 4612
  286.2 136.9 %collective-permute-start.4 = (bf16[3072,512]{0,1:T(8,128)(2,1)}, bf16[3072,512]{0,1:T(8,128)(2,1)}, u32[]{:S(2)}, u32[]{:S(2)}) collective-permute-start(bf16[3072,512]{0,1:T(8,128)(2,1)} %maximum_select_fusion.1), channel_id=1, source_target_pairs={{0,256},{16,272},{32,288},{48,304},{64,320},{80,336},{96,352},{112... | collective-permute-start | bytes 9437192 | tf_op jit(solution)/shard_map/ppermute | solution.py:144
  431.8 6.9 copy-start.1
  439.1 177.8 %copy-start.9 = (bf16[192,128]{1,0:T(8,128)(2,1)S(1)}, bf16[192,128]{1,0:T(8,128)(2,1)}, u32[]{:S(2)}) copy-start(bf16[192,128]{1,0:T(8,128)(2,1)} %param.35) | copy-start | bytes 147460
  439.1 177.8 %copy-start.14 = (f32[128]{0:T(128)S(1)}, f32[128]{0:T(128)}, u32[]{:S(2)}) copy-start(f32[128]{0:T(128)} %param.36) | copy-start | bytes 1540
  439.1 191.7 %copy-start.11 = (f32[128]{0:T(128)S(1)}, f32[128]{0:T(128)}, u32[]{:S(2)}) copy-start(f32[128]{0:T(128)} %param.37) | copy-start | bytes 1540
  440.2 298.3 %copy-start.4 = (bf16[128,512]{1,0:T(8,128)(2,1)S(1)}, bf16[128,512]{1,0:T(8,128)(2,1)}, u32[]{:S(2)}) copy-start(bf16[128,512]{1,0:T(8,128)(2,1)} %param.43) | copy-start | bytes 393220
  440.2 299.3 %copy-start.5 = (bf16[128,512]{1,0:T(8,128)(2,1)S(1)}, bf16[128,512]{1,0:T(8,128)(2,1)}, u32[]{:S(2)}) copy-start(bf16[128,512]{1,0:T(8,128)(2,1)} %param.44) | copy-start | bytes 393220
  440.2 315.4 %copy-start.2 = (bf16[4,128,512]{2,1,0:T(8,128)(2,1)S(1)}, bf16[4,128,512]{2,1,0:T(8,128)(2,1)}, u32[]{:S(2)}) copy-start(bf16[4,128,512]{2,1,0:T(8,128)(2,1)} %param.40) | copy-start | bytes 1572868
  440.2 163.3 %all-to-all-start = ((bf16[16,192,128]{2,1,0:T(8,128)(2,1)}), bf16[16,192,128]{2,1,0:T(8,128)(2,1)S(1)}, u32[]{:S(2)}, u32[]{:S(2)}) async-start(bf16[16,192,128]{2,1,0:T(8,128)(2,1)} %bitcast.107), calls=%async_computation | async-start | bytes 1572864 | tf_op jit(solution)/shard_map/all_to_all | solution.py:20
  592.2 164.6 %copy-start.3 = (bf16[4,128,512]{2,1,0:T(8,128)(2,1)S(1)}, bf16[4,128,512]{2,1,0:T(8,128)(2,1)}, u32[]{:S(2)}) copy-start(bf16[4,128,512]{2,1,0:T(8,128)(2,1)} %param.41) | copy-start | bytes 1572868
  631.2 233.2 %copy-start.15 = (bf16[4,512,128]{2,1,0:T(8,128)(2,1)S(1)}, bf16[4,512,128]{2,1,0:T(8,128)(2,1)}, u32[]{:S(2)}) copy-start(bf16[4,512,128]{2,1,0:T(8,128)(2,1)} %param.42) | copy-start | bytes 1572868
  632.0 123.6 %all-to-all-start.1 = ((bf16[32,4,5,128]{3,1,2,0:T(4,128)(2,1)}), bf16[32,4,5,128]{3,1,2,0:T(4,128)(2,1)S(1)}, u32[]{:S(2)}, u32[]{:S(2)}) async-start(bf16[32,4,5,128]{3,1,2,0:T(4,128)(2,1)} %copy.155), calls=%async_computation.1 | async-start | bytes 327680 | tf_op jit(solution)/shard_map/all_to_all | solution.py:203
  738.5 125.9 %all-reduce.3.cloned.1.call-start = ((), (), s32[]{:S(2)}) async-start(), calls=%async_computation.3 | async-start | bytes 3407872 | tf_op jit(solution)/shard_map/psum | solution.py:207
  864.4 17.7 %copy-start.13 = (f32[192,2]{0,1:T(2,128)S(1)}, f32[192,2]{0,1:T(2,128)}, u32[]{:S(2)}) copy-start(f32[192,2]{0,1:T(2,128)} %param.39) | copy-start | bytes 4612
  864.4 37.1 %copy-start.16 = (bf16[192,512]{1,0:T(8,128)(2,1)S(1)}, bf16[192,512]{1,0:T(8,128)(2,1)}, u32[]{:S(2)}) copy-start(bf16[192,512]{1,0:T(8,128)(2,1)} %get-tuple-element.357) | copy-start | bytes 589828
  864.4 37.1 %copy-start.17 = (bf16[192,512]{1,0:T(8,128)(2,1)S(1)}, bf16[192,512]{1,0:T(8,128)(2,1)}, u32[]{:S(2)}) copy-start(bf16[192,512]{1,0:T(8,128)(2,1)} %get-tuple-element.358) | copy-start | bytes 589828
  864.4 37.1 %copy-start.18 = (bf16[512,128]{1,0:T(8,128)(2,1)S(1)}, bf16[512,128]{1,0:T(8,128)(2,1)}, u32[]{:S(2)}) copy-start(bf16[512,128]{1,0:T(8,128)(2,1)} %param.45) | copy-start | bytes 393220
  867.1 31.7 %all-to-all-start.2 = ((bf16[32,4,5,128]{3,1,2,0:T(4,128)(2,1)}), bf16[32,4,5,128]{3,1,2,0:T(4,128)(2,1)S(1)}, u32[]{:S(2)}, u32[]{:S(2)}) async-start(bf16[32,4,5,128]{3,1,2,0:T(4,128)(2,1)} %copy.158), calls=%async_computation.2 | async-start | bytes 327680 | tf_op jit(solution)/shard_map/all_to_all | solution.py:210
Sparse Core Ops, SparseCore 0:
  758.1 106.2 all-reduce.2
